TPU v7x, 32 devices: a whole 2x2x4 slice. The times are simulated.
32 devices in a mesh: sp: 8 (over z, y), tp: 4 (over x, core).
Axes of the slice: x: 2, y: 2, z: 4, core: 2. Of those that a mesh axis runs over, the one named last changes fastest.
Arguments:
- tokens: bfloat16 [2048, 4096], P(('sp', 'tp')), may hold values from -6 to 6
- norm_gain: float32 [4096], replicated, may hold values from 0.1 to 1.9
- w_query: bfloat16 [4096, 1024], P(None, 'tp'), may hold values from -0.25 to 0.25
- w_key: bfloat16 [4096, 512], P(None, 'tp'), may hold values from -0.09375 to 0.09375
- w_value: bfloat16 [4096, 512], P(None, 'tp'), may hold values from -0.09375 to 0.09375
- score_shift: float32 [8], P('tp'), may hold values from -15 to -8
- w_conv_b: bfloat16 [4096, 1024], P(None, 'tp'), may hold values from -0.09375 to 0.09375
- w_conv_c: bfloat16 [4096, 1024], P(None, 'tp'), may hold values from -0.09375 to 0.09375
- w_conv_u: bfloat16 [4096, 1024], P(None, 'tp'), may hold values from -0.09375 to 0.09375
- conv_kernel: float32 [3, 1024], P(None, 'tp'), may hold values from -3.5 to 3.5
- w_out_att: bfloat16 [4096, 1024], P('sp', 'tp'), may hold values from -0.75 to 0.75
- w_out_conv: bfloat16 [4096, 1024], P('sp', 'tp'), may hold values from -0.1875 to 0.1875
Outputs:
- mixed: bfloat16 [2048, 4096], P(('sp', 'tp'))
- log_weight: float32 [2048, 8], P('sp', 'tp')
All inputs are finite; a program needn't handle non-finite values.
Results may differ from a plain program's by a relative error of at most 0.017.
Values may be sent and summed in bfloat16 or wider, within the bound.
A program may use at most 128 MiB of HBM per device.

v0:
```python
import jax
import jax.numpy as jnp
from jax import lax
from jax.sharding import PartitionSpec as P

HEAD_DIM = 128
CONV_K = 3
KEY_BLOCK = 1024


def swapped(block, axis, stride):
    count = lax.axis_size(axis)
    route = []
    for low in range(count):
        high = low | 1 << stride
        if high != low and high < count:
            route += [(low, high), (high, low)]
    return lax.ppermute(block, axis, route)


def shifted(value, axis, steps):
    count = lax.axis_size(axis)
    leading, last = (max(0, -steps), min(count, count - steps))
    return lax.ppermute(value, axis, [(source, source + steps) for source in range(leading, last)])


def normalize(tokens, norm_gain):
    widened = tokens.astype(jnp.float32)
    inverse = lax.rsqrt(jnp.mean(widened * widened, axis=-1, keepdims=True) + 1e-06)
    return (widened * inverse * norm_gain).astype(jnp.bfloat16)


def block_terms(grouped_q, key_block, value_block, shifts, query_pos, key_first):
    scores = jnp.einsum("qhgd,khd->qhgk", grouped_q, key_block, preferred_element_type=jnp.float32)
    scores = scores * HEAD_DIM ** (-0.5) + shifts[None, :, :, None]
    key_pos = key_first + jnp.arange(KEY_BLOCK, dtype=jnp.int32)
    causal = key_pos[None, None, None, :] < query_pos[:, None, None, None]
    soft = jnp.where(causal, jax.nn.softplus(scores), 0.0)
    after_sum = lax.cumsum(soft, axis=3, reverse=True) - soft
    relative = jnp.where(causal, jnp.exp(jax.nn.log_sigmoid(scores) - after_sum), 0.0).astype(
        jnp.bfloat16
    )
    partial_value = jnp.einsum(
        "qhgk,khd->qhgd", relative, value_block, preferred_element_type=jnp.float32
    )
    return (partial_value, jnp.sum(soft, axis=3))


def attend(grouped_q, query_pos, key_whole, value_whole, shifts):
    row_count, kv_local, grouping, head_size = grouped_q.shape
    last_block = jnp.max(query_pos) // KEY_BLOCK

    def visit(step, carry):
        accum, suffix = carry
        block_no = last_block - step
        key_first = block_no * KEY_BLOCK
        key_block = lax.dynamic_slice_in_dim(key_whole, key_first, KEY_BLOCK, 0).reshape(
            KEY_BLOCK, kv_local, head_size
        )
        value_block = lax.dynamic_slice_in_dim(value_whole, key_first, KEY_BLOCK, 0).reshape(
            KEY_BLOCK, kv_local, head_size
        )
        partial_value, total = block_terms(
            grouped_q, key_block, value_block, shifts, query_pos, key_first
        )
        accum = accum + jnp.exp(-suffix)[..., None] * partial_value
        return (accum, suffix + total)

    start = (
        jnp.zeros((row_count, kv_local, grouping, head_size), jnp.float32),
        jnp.zeros((row_count, kv_local, grouping), jnp.float32),
    )
    accum, suffix = lax.fori_loop(0, last_block + 1, visit, start)
    return (
        accum.reshape(row_count, kv_local * grouping * head_size),
        suffix.reshape(row_count, kv_local * grouping),
    )


def mirror_queries(payload):
    for bit in range(lax.axis_size("sp").bit_length() - 1):
        payload = swapped(payload, "sp", bit)
    return payload


def mirror_results(payload):
    for bit in range(lax.axis_size("sp").bit_length() - 1):
        payload = (
            swapped(payload[0].astype(jnp.bfloat16), "sp", bit).astype(jnp.float32),
            swapped(payload[1].astype(jnp.bfloat16), "sp", bit).astype(jnp.float32),
        )
    return payload


def local(
    tokens,
    norm_gain,
    w_query,
    w_key,
    w_value,
    score_shift,
    w_conv_b,
    w_conv_c,
    w_conv_u,
    conv_kernel,
    w_out_att,
    w_out_conv,
):
    weights = (w_query, w_key, w_value, w_conv_b, w_conv_c, w_conv_u)

    def project(rows_in):
        normed = normalize(rows_in, norm_gain)
        return jnp.concatenate(
            [
                jnp.dot(normed, weight, preferred_element_type=jnp.float32).astype(jnp.bfloat16)
                for weight in weights
            ],
            axis=1,
        )

    projected = project(lax.all_gather(tokens, "tp", axis=0, tiled=True))
    widths = [weight.shape[1] for weight in weights]
    edges = [0]
    for width in widths:
        edges.append(edges[-1] + width)
    queries, keys, values, gate_b, gate_c, inputs_u = [
        projected[:, edges[pos] : edges[pos + 1]] for pos in range(6)
    ]
    tok_count = projected.shape[0]
    conv_local = gate_b.shape[1]
    products = (gate_c.astype(jnp.float32) * inputs_u.astype(jnp.float32)).astype(jnp.bfloat16)
    previous = shifted(products[tok_count - (CONV_K - 1) :], "sp", 1)
    key_whole, value_whole = (
        lax.all_gather(keys, "sp", axis=0, tiled=True),
        lax.all_gather(values, "sp", axis=0, tiled=True),
    )
    local_heads = queries.shape[1] // HEAD_DIM
    kv_local = keys.shape[1] // HEAD_DIM
    grouping = local_heads // kv_local
    shifts = score_shift.reshape(kv_local, grouping)
    sp_count = lax.axis_size("sp")
    sp_index = lax.axis_index("sp")
    half = tok_count // 2
    own_q = queries[:half].reshape(half, kv_local, grouping, HEAD_DIM)
    own_pos = sp_index * tok_count + jnp.arange(half, dtype=jnp.int32)
    own_att, own_sums = attend(own_q, own_pos, key_whole, value_whole, shifts)
    other_q = mirror_queries(queries[half:]).reshape(tok_count - half, kv_local, grouping, HEAD_DIM)
    other_pos = (
        (sp_count - 1 - sp_index) * tok_count + half + jnp.arange(tok_count - half, dtype=jnp.int32)
    )
    other_att, other_sums = attend(other_q, other_pos, key_whole, value_whole, shifts)
    back_att, back_sums = mirror_results((other_att, other_sums))
    attended_f = jnp.concatenate([own_att, back_att], axis=0)
    sums_all = jnp.concatenate([own_sums, back_sums], axis=0)
    attended = attended_f.astype(jnp.bfloat16)
    log_weight = jnp.log(jnp.maximum(-jnp.expm1(-sums_all), 0.05))
    extended = jnp.concatenate([previous, products], axis=0)
    summed = jnp.zeros((tok_count, conv_local), jnp.float32)
    for tap in range(CONV_K):
        summed = summed + conv_kernel[tap][None, :] * extended[tap : tap + tok_count].astype(
            jnp.float32
        )
    convolved = (gate_b.astype(jnp.float32) * summed).astype(jnp.bfloat16)
    contract = (((1,), (1,)), ((), ()))
    pieces = lax.all_gather((w_out_att, w_out_conv), "sp", axis=0, tiled=True)
    result = lax.dot_general(attended, pieces[0], contract, preferred_element_type=jnp.float32)
    share = result + lax.dot_general(
        convolved, pieces[1], contract, preferred_element_type=jnp.float32
    )
    rounded = share.astype(jnp.bfloat16).astype(jnp.float32)
    mixed = lax.psum_scatter(rounded.astype(jnp.bfloat16), "tp", scatter_dimension=0, tiled=True)
    return (mixed, log_weight)


def solution(mesh):
    return jax.shard_map(
        local,
        mesh=mesh,
        in_specs=(
            P(("sp", "tp"), None),
            P(),
            P(None, "tp"),
            P(None, "tp"),
            P(None, "tp"),
            P("tp"),
            P(None, "tp"),
            P(None, "tp"),
            P(None, "tp"),
            P(None, "tp"),
            P("sp", "tp"),
            P("sp", "tp"),
        ),
        out_specs=(P(("sp", "tp"), None), P("sp", "tp")),
        check_vma=False,
    )
```

profile of v0, /device:TPU:17, one launch (start us, length us, event | category | flops | bytes accessed | tf_op | source)
XLA Modules:
  0.0 193.6 jit_solution(12022105615553564514)
XLA Ops:
  7.2 0.7 all-gather.4.cloned.1.call-update
  8.0 0.7 all-gather.8.cloned.1.call-update
  8.7 0.7 all-gather.6.cloned.1.call-update
  9.5 0.6 add_reduce_fusion
  12.0 0.7 add_reduce_fusion.1
  15.9 0.8 fusion.88
  16.7 16.9 %all-gather.4.cloned.1.call-done = bf16[256,4096]{1,0:T(8,128)(2,1)} async-done(((bf16[64,4096]{1,0:T(8,128)(2,1)}), bf16[256,4096]{1,0:T(8,128)(2,1)}) %all-gather.4.cloned.1.call-update) | async-done | bytes 2097168 | tf_op jit(solution)/shard_map/all_gather | solution.py:121
  33.6 2.2 %fusion.53 = f32[256]{0:T(256)S(1)} fusion(bf16[256,4096]{1,0:T(8,128)(2,1)} %all-gather.4.cloned.1.call-done), kind=kLoop, calls=%fused_computation.78 | loop fusion | flops 3145472 | bytes 2098176 | tf_op jit(solution)/shard_map/reduce_sum | solution.py:29
  35.9 0.6 fusion.55
  36.5 0.6 copy-done.9
  37.1 0.7 convolution_convert_fusion.5
  37.8 1.6 copy-done.7
  39.5 1.0 convolution_convert_fusion.3
  40.4 1.3 collective-permute-start
  41.7 1.4 fusion.59
  43.1 0.7 convolution_convert_fusion.4
  43.8 1.3 collective-permute-start.1
  45.1 24.1 %all_gather.16 = bf16[2048,128]{1,0:T(8,128)(2,1)S(1)} all-gather(bf16[256,128]{1,0:T(8,128)(2,1)S(1)} %convolution_convert_fusion.5), channel_id=1, replica_groups=mesh['sp'=8,'tp'=4] {'sp'}, dimensions={0}, use_global_device_ids=true | all-gather | bytes 589824 | tf_op jit(solution)/shard_map/all_gather | solution.py:135
  69.2 4.3 %collective-permute-start.2 = (bf16[128,256]{0,1:T(8,128)(2,1)S(1)}, bf16[128,256]{0,1:T(8,128)(2,1)S(1)}, u32[]{:S(2)}, u32[]{:S(2)}) collective-permute-start(bf16[128,256]{0,1:T(8,128)(2,1)S(1)} %collective-permute-done.1), channel_id=1, source_target_pairs={{0,16},{16,0},{4,20},{20,4},{8,24},{24,8},{12,28},{28,12},{1,17},{... | collective-permute-start | bytes 196616 | tf_op jit(solution)/shard_map/ppermute | solution.py:18
  73.5 22.9 %all_gather.17 = bf16[2048,128]{1,0:T(8,128)(2,1)S(1)} all-gather(bf16[256,128]{1,0:T(8,128)(2,1)S(1)} %convolution_convert_fusion.4), channel_id=1, replica_groups=mesh['sp'=8,'tp'=4] {'sp'}, dimensions={0}, use_global_device_ids=true | all-gather | bytes 589824 | tf_op jit(solution)/shard_map/all_gather | solution.py:134
  96.3 1.0 copy.20
  97.4 0.1 copy.23
  97.5 7.7 %while.27 = (s32[]{:T(128)}, f32[128,1,2,128]{0,3,2,1:T(8,128)S(1)}, f32[128,1,2]{0,2,1:T(2,128)S(1)}, s32[]{:T(128)}, s32[]{:T(128)}, /*index=5*/bf16[2048,128]...) while((s32[]{:T(128)}, ...), condition=%wide.region_12.13_spmd.clone, body=%wide.region_8.12_spmd.clone.sunk | while | flops 175588480 | bytes 23864196 | solution.py:73
  97.6 0.2 broadcast_compare_fusion.5
  97.8 1.9 fusion.127
  99.7 2.5 %fusion.128 = f32[128,1,2,8,128]{0,3,2,1,4:T(8,128)S(1)} fusion(f32[128,1,2,8,128]{0,4,3,2,1:T(8,128)S(1)} %bitcast.178), kind=kOutput, calls=%fused_computation.56.clone.1 | output fusion | flops 33292288 | bytes 2097152 | tf_op jit(solution)/shard_map/reduce-window.2
  102.3 0.1 broadcast.117
  102.3 0.3 copy.37
  102.7 0.8 copy-done.2
  103.5 1.5 fusion.129
  104.9 0.2 fusion.130
  105.3 0.7 collective-permute-start.3
  105.9 3.0 %fusion.58 = bf16[256,256]{1,0:T(8,128)(2,1)S(1)} fusion(f32[256,256]{1,0:T(8,128)} %fusion.59, bf16[256,4096]{1,0:T(8,128)(2,1)} %copy-done.1, bf16[4096,256]{1,0:T(8,128)(2,1)} %param.24), kind=kOutput, calls=%fused_computation.84 | convolution fusion | flops 537133056 | bytes 4587520 | tf_op jit(solution)/shard_map/dot_general | solution.py:115
  108.9 0.1 copy.21
  109.1 2.7 %collective-permute-start.6 = (bf16[2,256]{1,0:T(2,128)(2,1)S(1)}, bf16[2,256]{1,0:T(2,128)(2,1)S(1)}, u32[]{:S(2)}, u32[]{:S(2)}) collective-permute-start(bf16[2,256]{1,0:T(2,128)(2,1)S(1)} %slice.54), channel_id=1, source_target_pairs={{0,4},{4,8},{8,12},{12,16},{16,20},{20,24},{24,28},{1,5},{5,9},{9,... | collective-permute-start | bytes 3080 | tf_op jit(solution)/shard_map/ppermute | solution.py:24
  111.8 2.3 %collective-permute-start.4 = (bf16[128,256]{0,1:T(8,128)(2,1)}, bf16[128,256]{0,1:T(8,128)(2,1)}, u32[]{:S(2)}, u32[]{:S(2)}) collective-permute-start(bf16[128,256]{0,1:T(8,128)(2,1)} %collective-permute-done.3), channel_id=1, source_target_pairs={{0,8},{8,0},{4,12},{12,4},{16,24},{24,16},{20,28},{28,20},{1,9},{9... | collective-permute-start | bytes 196616 | tf_op jit(solution)/shard_map/ppermute | solution.py:18
  114.1 15.6 %while.26 = (s32[]{:T(128)}, f32[128,1,2,128]{0,3,2,1:T(8,128)S(1)}, f32[128,1,2]{0,2,1:T(2,128)S(1)}, s32[]{:T(128)}, s32[]{:T(128)}, /*index=5*/bf16[2048,128]...) while((s32[]{:T(128)}, ...), condition=%wide.region_6.7_spmd.clone, body=%wide.region_2.6_spmd.clone.sunk | while | flops 175588480 | bytes 23864196 | solution.py:73
  114.4 0.2 broadcast_compare_fusion.4
  114.6 1.8 fusion.120
  116.4 2.5 %fusion.121 = f32[128,1,2,8,128]{0,3,2,1,4:T(8,128)S(1)} fusion(f32[128,1,2,8,128]{0,4,3,2,1:T(8,128)S(1)} %bitcast.179), kind=kOutput, calls=%fused_computation.20.clone.1 | output fusion | flops 33292288 | bytes 2097152 | tf_op jit(solution)/shard_map/reduce-window
  119.0 0.1 broadcast.116
  119.1 0.3 copy.35
  119.4 0.8 copy-done.3
  120.2 1.5 fusion.122
  121.7 0.2 fusion.123
  122.0 0.2 broadcast_compare_fusion.4
  122.3 1.8 fusion.120
  124.1 2.5 %fusion.121 = f32[128,1,2,8,128]{0,3,2,1,4:T(8,128)S(1)} fusion(f32[128,1,2,8,128]{0,4,3,2,1:T(8,128)S(1)} %bitcast.179), kind=kOutput, calls=%fused_computation.20.clone.1 | output fusion | flops 33292288 | bytes 2097152 | tf_op jit(solution)/shard_map/reduce-window
  126.8 0.3 copy.35
  127.1 0.8 copy-done.3
  127.9 1.5 fusion.122
  129.4 0.2 fusion.123
  129.7 1.9 collective-permute-start.5
  131.6 6.6 %fusion.63 = f32[256,4096]{1,0:T(8,128)} fusion(bf16[4096,256]{1,0:T(8,128)(2,1)} %all-gather.8.cloned.1.call-done, bf16[256,4096]{1,0:T(8,128)(2,1)} %copy-done.1, bf16[4096,256]{1,0:T(8,128)(2,1)S(1)} %copy-done, bf16[256,256]{1,0:T(8,128)(2,1)} %copy-done.11, bf16[2,256]{1,0:T(2,128)(2,1)S(1)} %collective-permute-done.6, f32[256]{0:T(256)S(1)} %bitcast.186, ...), kind=kOutput, calls=%fused_computation.92 | convolution fusion | flops 1074921472 | bytes 10620928 | tf_op jit(solution)/shard_map/dot_general | solution.py:167
  138.2 3.6 %all-gather.6.cloned.1.call-done = bf16[4096,256]{1,0:T(8,128)(2,1)} async-done(((bf16[512,256]{1,0:T(8,128)(2,1)}), bf16[4096,256]{1,0:T(8,128)(2,1)}) %all-gather.6.cloned.1.call-update) | async-done | bytes 2097168 | tf_op jit(solution)/shard_map/all_gather | solution.py:165
  141.8 4.9 %fusion.52 = bf16[256,4096]{1,0:T(8,128)(2,1)} fusion(f32[256,4096]{1,0:T(8,128)} %fusion.63, bf16[4096,256]{1,0:T(8,128)(2,1)} %all-gather.6.cloned.1.call-done, bf16[128,256]{0,1:T(8,128)(2,1)S(1)} %collective-permute-done.5, bf16[128,256]{0,1:T(8,128)(2,1)S(1)} %bitcast.180), kind=kOutput, calls=%fused_computation.77 | convolution fusion | flops 539230208 | bytes 8519680 | tf_op jit(solution)/shard_map/dot_general | solution.py:166
  146.8 0.2 collective-permute-start.7
  146.9 2.3 %collective-permute-done.7 = bf16[128,2]{0,1:T(2,128)(2,1)S(1)} collective-permute-done((bf16[128,2]{0,1:T(2,128)(2,1)S(1)}, bf16[128,2]{0,1:T(2,128)(2,1)S(1)}, u32[]{:S(2)}, u32[]{:S(2)}) %collective-permute-start.7) | collective-permute-done | bytes 544 | tf_op jit(solution)/shard_map/ppermute | solution.py:18
  149.3 0.5 collective-permute-start.8
  149.7 2.0 %collective-permute-done.8 = bf16[128,2]{0,1:T(2,128)(2,1)S(1)} collective-permute-done((bf16[128,2]{0,1:T(2,128)(2,1)S(1)}, bf16[128,2]{0,1:T(2,128)(2,1)S(1)}, u32[]{:S(2)}, u32[]{:S(2)}) %collective-permute-start.8) | collective-permute-done | bytes 544 | tf_op jit(solution)/shard_map/ppermute | solution.py:18
  151.7 1.6 collective-permute-start.9
  153.3 1.7 collective-permute-done.9
  155.0 0.6 fusion.84
  155.6 31.4 %reduce-scatter.2.cloned.1.call-done = bf16[64,4096]{1,0:T(8,128)(2,1)} async-done(((bf16[256,4096]{1,0:T(8,128)(2,1)}), bf16[64,4096]{1,0:T(8,128)(2,1)}) %reduce-scatter.2.cloned.1.call-update) | async-done | bytes 524304 | tf_op jit(solution)/shard_map/reduce_scatter | solution.py:171
  (94 shorter events, 0.6 us)
Async XLA Ops:
  7.2 124.4 %copy-start = (bf16[4096,256]{1,0:T(8,128)(2,1)S(1)}, bf16[4096,256]{1,0:T(8,128)(2,1)}, u32[]{:S(2)}) copy-start(bf16[4096,256]{1,0:T(8,128)(2,1)} %param.22) | copy-start | bytes 6291460
  7.2 28.7 %copy-start.20 = (f32[4096]{0:T(1024)S(1)}, f32[4096]{0:T(1024)}, u32[]{:S(2)}) copy-start(f32[4096]{0:T(1024)} %param.17) | copy-start | bytes 49156
  7.2 26.4 %all-gather.4.cloned.1.call-start = ((), (), s32[]{:S(2)}) async-start(), calls=%async_computation.1 | async-start | bytes 2621440 | tf_op jit(solution)/shard_map/all_gather | solution.py:121
  7.9 123.7 %all-gather.8.cloned.1.call-start = ((), (), s32[]{:S(2)}) async-start(), calls=%async_computation.3 | async-start | bytes 2359296 | tf_op jit(solution)/shard_map/all_gather | solution.py:165
  8.7 133.1 %all-gather.6.cloned.1.call-start = ((), (), s32[]{:S(2)}) async-start(), calls=%async_computation.2 | async-start | bytes 2359296 | tf_op jit(solution)/shard_map/all_gather | solution.py:165
  9.4 177.6 %reduce-scatter.2.cloned.1.call-start = ((), (), s32[]{:S(2)}) async-start(), calls=%async_computation.4 | async-start | bytes 2621440 | tf_op jit(solution)/shard_map/reduce_scatter | solution.py:171
  33.6 2.3 %copy-start.6 = (bf16[256,4096]{1,0:T(8,128)(2,1)S(1)}, bf16[256,4096]{1,0:T(8,128)(2,1)}, u32[]{:S(2)}) copy-start(bf16[256,4096]{1,0:T(8,128)(2,1)} %all-gather.4.cloned.1.call-done) | copy-start | bytes 6291460
  35.9 1.2 copy-start.9
  37.1 6.0 %copy-start.1 = (bf16[256,4096]{1,0:T(8,128)(2,1)}, bf16[256,4096]{1,0:T(8,128)(2,1)S(1)}, u32[]{:S(2)}) copy-start(bf16[256,4096]{1,0:T(8,128)(2,1)S(1)} %fusion.55) | copy-start | bytes 6291460
  37.1 2.3 %copy-start.7 = (bf16[4096,256]{1,0:T(8,128)(2,1)S(1)}, bf16[4096,256]{1,0:T(8,128)(2,1)}, u32[]{:S(2)}) copy-start(bf16[4096,256]{1,0:T(8,128)(2,1)} %param.18) | copy-start | bytes 6291460
  39.5 2.3 %copy-start.8 = (bf16[4096,256]{1,0:T(8,128)(2,1)S(1)}, bf16[4096,256]{1,0:T(8,128)(2,1)}, u32[]{:S(2)}) copy-start(bf16[4096,256]{1,0:T(8,128)(2,1)} %param.23) | copy-start | bytes 6291460
  40.4 2.7 %copy-start.10 = (bf16[4096,128]{1,0:T(8,128)(2,1)S(1)}, bf16[4096,128]{1,0:T(8,128)(2,1)}, u32[]{:S(2)}) copy-start(bf16[4096,128]{1,0:T(8,128)(2,1)} %param.19) | copy-start | bytes 3145732
  40.4 3.4 %collective-permute-start = (bf16[128,256]{0,1:T(8,128)(2,1)S(1)}, bf16[128,256]{0,1:T(8,128)(2,1)S(1)}, u32[]{:S(2)}, u32[]{:S(2)}) collective-permute-start(bf16[128,256]{0,1:T(8,128)(2,1)S(1)} %get-tuple-element.233), channel_id=1, source_target_pairs={{0,4},{4,0},{8,12},{12,8},{16,20},{20,16},{24,28},{28,24},{1,5},{5... | collective-permute-start | bytes 196616 | tf_op jit(solution)/shard_map/ppermute | solution.py:18
  43.1 54.4 %copy-start.21 = (f32[2]{0:T(128)S(1)}, f32[2]{0:T(128)}, u32[]{:S(2)}) copy-start(f32[2]{0:T(128)} %param.21) | copy-start | bytes 28
  43.8 25.3 %collective-permute-start.1 = (bf16[128,256]{0,1:T(8,128)(2,1)S(1)}, bf16[128,256]{0,1:T(8,128)(2,1)S(1)}, u32[]{:S(2)}, u32[]{:S(2)}) collective-permute-start(bf16[128,256]{0,1:T(8,128)(2,1)S(1)} %collective-permute-done), channel_id=1, source_target_pairs={{0,8},{8,0},{4,12},{12,4},{16,24},{24,16},{20,28},{28,20},{1,9},{9... | collective-permute-start | bytes 196616 | tf_op jit(solution)/shard_map/ppermute | solution.py:18
  69.2 28.2 %collective-permute-start.2 = (bf16[128,256]{0,1:T(8,128)(2,1)S(1)}, bf16[128,256]{0,1:T(8,128)(2,1)S(1)}, u32[]{:S(2)}, u32[]{:S(2)}) collective-permute-start(bf16[128,256]{0,1:T(8,128)(2,1)S(1)} %collective-permute-done.1), channel_id=1, source_target_pairs={{0,16},{16,0},{4,20},{20,4},{8,24},{24,8},{12,28},{28,12},{1,17},{... | collective-permute-start | bytes 196616 | tf_op jit(solution)/shard_map/ppermute | solution.py:18
  97.5 2.1 %copy-start.12 = (bf16[2048,128]{1,0:T(8,128)(2,1)}, bf16[2048,128]{1,0:T(8,128)(2,1)S(1)}, u32[]{:S(2)}) copy-start(bf16[2048,128]{1,0:T(8,128)(2,1)S(1)} %get-tuple-element.417) | copy-start | bytes 1572868 | tf_op jit(solution)/shard_map/while
  97.6 2.1 %copy-start.18 = (bf16[128,1,2,128]{3,0,2,1:T(8,128)(2,1)}, bf16[128,1,2,128]{3,0,2,1:T(8,128)(2,1)S(1)}, u32[]{:S(2)}) copy-start(bf16[128,1,2,128]{3,0,2,1:T(8,128)(2,1)S(1)} %get-tuple-element.418) | copy-start | bytes 196612 | tf_op jit(solution)/shard_map/while
  102.2 1.2 copy-start.2
  102.7 2.3 %copy-start.4 = (bf16[2048,128]{0,1:T(8,128)(2,1)S(1)}, bf16[2048,128]{0,1:T(8,128)(2,1)}, u32[]{:S(2)}) copy-start(bf16[2048,128]{0,1:T(8,128)(2,1)} %get-tuple-element.416) | copy-start | bytes 1572868 | tf_op jit(solution)/shard_map/while
  103.5 1.7 copy-start.13
  103.5 1.8 copy-start.19
  105.3 6.6 %collective-permute-start.3 = (bf16[128,256]{0,1:T(8,128)(2,1)S(1)}, bf16[128,256]{0,1:T(8,128)(2,1)}, u32[]{:S(2)}, u32[]{:S(2)}) collective-permute-start(bf16[128,256]{0,1:T(8,128)(2,1)S(1)} %bitcast.182), channel_id=1, source_target_pairs={{0,4},{4,0},{8,12},{12,8},{16,20},{20,16},{24,28},{28,24},{1,5},{5... | collective-permute-start | bytes 196616 | tf_op jit(solution)/shard_map/ppermute | solution.py:18
  108.9 5.2 %copy-start.11 = (bf16[256,256]{1,0:T(8,128)(2,1)}, bf16[256,256]{1,0:T(8,128)(2,1)S(1)}, u32[]{:S(2)}) copy-start(bf16[256,256]{1,0:T(8,128)(2,1)S(1)} %fusion.58) | copy-start | bytes 393220
  109.1 22.5 %collective-permute-start.6 = (bf16[2,256]{1,0:T(2,128)(2,1)S(1)}, bf16[2,256]{1,0:T(2,128)(2,1)S(1)}, u32[]{:S(2)}, u32[]{:S(2)}) collective-permute-start(bf16[2,256]{1,0:T(2,128)(2,1)S(1)} %slice.54), channel_id=1, source_target_pairs={{0,4},{4,8},{8,12},{12,16},{16,20},{20,24},{24,28},{1,5},{5,9},{9,... | collective-permute-start | bytes 3080 | tf_op jit(solution)/shard_map/ppermute | solution.py:24
  111.8 17.9 %collective-permute-start.4 = (bf16[128,256]{0,1:T(8,128)(2,1)}, bf16[128,256]{0,1:T(8,128)(2,1)}, u32[]{:S(2)}, u32[]{:S(2)}) collective-permute-start(bf16[128,256]{0,1:T(8,128)(2,1)} %collective-permute-done.3), channel_id=1, source_target_pairs={{0,8},{8,0},{4,12},{12,4},{16,24},{24,16},{20,28},{28,20},{1,9},{9... | collective-permute-start | bytes 196616 | tf_op jit(solution)/shard_map/ppermute | solution.py:18
  114.3 2.1 %copy-start.14 = (bf16[2048,128]{1,0:T(8,128)(2,1)}, bf16[2048,128]{1,0:T(8,128)(2,1)S(1)}, u32[]{:S(2)}) copy-start(bf16[2048,128]{1,0:T(8,128)(2,1)S(1)} %get-tuple-element.462) | copy-start | bytes 1572868 | tf_op jit(solution)/shard_map/while
  114.3 2.1 %copy-start.16 = (bf16[128,1,2,128]{3,0,2,1:T(8,128)(2,1)}, bf16[128,1,2,128]{3,0,2,1:T(8,128)(2,1)S(1)}, u32[]{:S(2)}) copy-start(bf16[128,1,2,128]{3,0,2,1:T(8,128)(2,1)S(1)} %get-tuple-element.463) | copy-start | bytes 196612 | tf_op jit(solution)/shard_map/while
  119.0 1.2 copy-start.3
  119.4 2.3 %copy-start.5 = (bf16[2048,128]{0,1:T(8,128)(2,1)S(1)}, bf16[2048,128]{0,1:T(8,128)(2,1)}, u32[]{:S(2)}) copy-start(bf16[2048,128]{0,1:T(8,128)(2,1)} %get-tuple-element.461) | copy-start | bytes 1572868 | tf_op jit(solution)/shard_map/while
  120.2 1.7 copy-start.15
  120.2 1.8 copy-start.17
  122.0 2.1 %copy-start.14 = (bf16[2048,128]{1,0:T(8,128)(2,1)}, bf16[2048,128]{1,0:T(8,128)(2,1)S(1)}, u32[]{:S(2)}) copy-start(bf16[2048,128]{1,0:T(8,128)(2,1)S(1)} %get-tuple-element.462) | copy-start | bytes 1572868 | tf_op jit(solution)/shard_map/while
  122.0 2.1 %copy-start.16 = (bf16[128,1,2,128]{3,0,2,1:T(8,128)(2,1)}, bf16[128,1,2,128]{3,0,2,1:T(8,128)(2,1)S(1)}, u32[]{:S(2)}) copy-start(bf16[128,1,2,128]{3,0,2,1:T(8,128)(2,1)S(1)} %get-tuple-element.463) | copy-start | bytes 196612 | tf_op jit(solution)/shard_map/while
  126.7 1.2 copy-start.3
  127.1 2.3 %copy-start.5 = (bf16[2048,128]{0,1:T(8,128)(2,1)S(1)}, bf16[2048,128]{0,1:T(8,128)(2,1)}, u32[]{:S(2)}) copy-start(bf16[2048,128]{0,1:T(8,128)(2,1)} %get-tuple-element.461) | copy-start | bytes 1572868 | tf_op jit(solution)/shard_map/while
  127.9 1.7 copy-start.15
  127.9 1.8 copy-start.17
  129.7 8.5 %collective-permute-start.5 = (bf16[128,256]{0,1:T(8,128)(2,1)}, bf16[128,256]{0,1:T(8,128)(2,1)S(1)}, u32[]{:S(2)}, u32[]{:S(2)}) collective-permute-start(bf16[128,256]{0,1:T(8,128)(2,1)} %collective-permute-done.4), channel_id=1, source_target_pairs={{0,16},{16,0},{4,20},{20,4},{8,24},{24,8},{12,28},{28,12},{1,17},{... | collective-permute-start | bytes 196616 | tf_op jit(solution)/shard_map/ppermute | solution.py:18
  146.8 2.5 %collective-permute-start.7 = (bf16[128,2]{0,1:T(2,128)(2,1)S(1)}, bf16[128,2]{0,1:T(2,128)(2,1)S(1)}, u32[]{:S(2)}, u32[]{:S(2)}) collective-permute-start(bf16[128,2]{0,1:T(2,128)(2,1)S(1)} %convert_bitcast_fusion), channel_id=1, source_target_pairs={{0,4},{4,0},{8,12},{12,8},{16,20},{20,16},{24,28},{28,24},{1,5},{5... | collective-permute-start | bytes 1544 | tf_op jit(solution)/shard_map/ppermute | solution.py:18
  149.3 2.4 %collective-permute-start.8 = (bf16[128,2]{0,1:T(2,128)(2,1)S(1)}, bf16[128,2]{0,1:T(2,128)(2,1)S(1)}, u32[]{:S(2)}, u32[]{:S(2)}) collective-permute-start(bf16[128,2]{0,1:T(2,128)(2,1)S(1)} %collective-permute-done.7), channel_id=1, source_target_pairs={{0,8},{8,0},{4,12},{12,4},{16,24},{24,16},{20,28},{28,20},{1,9},{9... | collective-permute-start | bytes 1544 | tf_op jit(solution)/shard_map/ppermute | solution.py:18
  151.7 3.3 %collective-permute-start.9 = (bf16[128,2]{0,1:T(2,128)(2,1)S(1)}, bf16[128,2]{0,1:T(2,128)(2,1)S(1)}, u32[]{:S(2)}, u32[]{:S(2)}) collective-permute-start(bf16[128,2]{0,1:T(2,128)(2,1)S(1)} %collective-permute-done.8), channel_id=1, source_target_pairs={{0,16},{16,0},{4,20},{20,4},{8,24},{24,8},{12,28},{28,12},{1,17},{... | collective-permute-start | bytes 1544 | tf_op jit(solution)/shard_map/ppermute | solution.py:18
Sparse Core Ops, SparseCore 0:
  9.6 24.0 all-gather.3
  35.7 55.5 all-gather.7
  93.5 48.2 all-gather.5
  146.9 40.0 reduce-scatter.1
where the time goes:
time: 196 us; the launch traced here: 194 us
  waiting for transfers between devices  60 us (31%)
  blocking collectives  46.9 us (24%)
  matrix products  24.6 us (13%)
  between operations  19.2 us (10%)
  other arithmetic  17.5 us (9%)
  starting transfers between devices  16.8 us (9%)
  local copies, waits for them, and re-layouts  7.98 us (4%)
    reduce_scatter x1, waiting for transfers between devices, local(): lax.psum_scatter(rounded.astype(jnp.bfloat16), 'tp', scatter_dimension=0,...  31.4 us
    all_gather x1, blocking collectives, local(): lax.all_gather(values, 'sp', axis=0, tiled=True)  24.1 us
    all_gather x1, blocking collectives, local(): lax.all_gather(keys, 'sp', axis=0, tiled=True)  22.9 us
    all_gather x1, waiting for transfers between devices, local(): projected = project(lax.all_gather(tokens, 'tp', axis=0, tiled=True))  16.9 us
    ppermute x9, starting transfers between devices, swapped(): return lax.ppermute(block, axis, route)  13.9 us
    another operation x7, other arithmetic  7.65 us
    dot_general x5, matrix products, project(): jnp.dot(normed, weight, preferred_element_type=jnp.float32)  6.71 us
    dot_general x1, matrix products, local(): lax.dot_general(convolved, pieces[1], contract, preferred_element_type=jn...  6.64 us
  transfers between devices with their start and end apart: 14, of which 6 were waited for; matrix products, arithmetic and copies ran while one was open for 21% of the time, Pallas kernels for 0%

commit v1 on v0

v1 whole, which is shorter than its diff:
```python
import functools

import jax
import jax.numpy as jnp
from jax import lax
from jax.experimental import pallas as pl
from jax.experimental.pallas import tpu as pltpu
from jax.sharding import PartitionSpec as P

HEAD_DIM = 128
CONV_K = 3
HALO = 16
F32 = jnp.float32
BF16 = jnp.bfloat16
MESH = pl.DeviceIdType.MESH
NT = (((1,), (1,)), ((), ()))


def softplus(z):
    u = jnp.exp(-jnp.abs(z))
    small = u * (1.0 - u * (0.5 - u * (1.0 / 3.0 - u * 0.25)))
    return jnp.maximum(z, 0.0) + jnp.where(u < 0.01, small, jnp.log(1.0 + u))


def kernel(
    n,
    tok_ref, gain_ref, wq_hbm, wk_hbm, wv_hbm, shift_ref, wb_hbm, wc_hbm, wu_hbm, taps_ref, woa_ref, woc_ref,
    out_ref, logw_ref,
    wq, wk, wv, wb, wc, wu, xall, normed, q_sc, kv, wo, gate_sc, prod_sc, prev, ext, attn, conv,
    snd, keep, d2d, xsnd, xrcv,
    load_sem, tok_ssem, tok_rsem, kv_sem, w_sem, halo_sem, d2d_sem, x_sem,
):
    sp = lax.axis_index("sp")
    t = lax.axis_index("tp")
    near = t + 1 - 2 * (t % 2)
    far = t + 2 - 4 * ((t // 2) % 2)
    diag = near + 2 - 4 * ((near // 2) % 2)
    pos = jnp.where(sp % 2 == 0, sp // 2, n - 1 - sp // 2)

    def ring(place):
        place = (place + 2 * n) % n
        return jnp.where(place < n // 2, 2 * place, 2 * (n - 1 - place) + 1)

    right, left = ring(pos + 1), ring(pos - 1)
    following, leading = (sp + 1) % n, (sp + n - 1) % n
    rows = tok_ref.shape[0]
    toks = 4 * rows
    half = rows // 2
    heads = q_sc.shape[1] // HEAD_DIM
    kv_cols = kv.shape[3]
    grouping = heads // (kv_cols // HEAD_DIM)

    loads = [
        pltpu.make_async_copy(src, dst, load_sem.at[i])
        for i, (src, dst) in enumerate(
            ((wk_hbm, wk), (wv_hbm, wv), (wq_hbm, wq), (wc_hbm, wc), (wu_hbm, wu), (wb_hbm, wb))
        )
    ]
    barrier = pltpu.get_barrier_semaphore()
    for place in (right, left, following, leading):
        pl.semaphore_signal(barrier, inc=1, device_id={"sp": place}, device_id_type=MESH)
    for place in (near, far):
        pl.semaphore_signal(barrier, inc=1, device_id={"tp": place}, device_id_type=MESH)
    for load in loads:
        load.start()
    pl.semaphore_wait(barrier, 6)

    def push(src, dst, ssem, rsem, who):
        return pltpu.make_async_remote_copy(
            src_ref=src, dst_ref=dst, send_sem=ssem, recv_sem=rsem, device_id=who, device_id_type=MESH
        )

    to_far = [
        push(tok_ref.at[pl.ds(c * half, half)], xall.at[t, pl.ds(c * half, half)], tok_ssem.at[c], tok_rsem.at[c], {"tp": far})
        for c in range(2)
    ]
    to_near = push(tok_ref, xall.at[t], tok_ssem.at[2], tok_rsem.at[2], {"tp": near})
    relay = [
        push(xall.at[far, pl.ds(c * half, half)], xall.at[far, pl.ds(c * half, half)], tok_ssem.at[3 + c], tok_rsem.at[3 + c], {"tp": near})
        for c in range(2)
    ]
    for copy in to_far:
        copy.start()
    to_near.start()

    def hop(buf, sem, way, k, own):
        step, chunk = k // 2 + 1, k % 2 if way == 0 else 1 - k % 2
        block = ring(pos - (step - 1)) if way == 0 else ring(pos + (step - 1))
        src = own[chunk] if (own is not None and step == 1) else buf.at[block, chunk]
        who = right if way == 0 else left
        return push(src, buf.at[block, chunk], sem.at[0, way, k], sem.at[1, way, k], {"sp": who})

    def open_ring(buf, sem, own):
        for k in range(min(2, n - 1)):
            for way in range(2):
                hop(buf, sem, way, k, own).start()

    def serve(buf, sem, own, step):
        for k in (2 * step - 2, 2 * step - 1):
            if k <= n - 2:
                for way in range(2):
                    hop(buf, sem, way, k, own).wait_recv()
                    if k + 2 <= n - 2:
                        hop(buf, sem, way, k + 2, own).start()

    own_w = (woa_ref, woc_ref)
    open_ring(wo, w_sem, own_w)

    def project(groups, offset):
        for i, g in enumerate(groups):
            x = (tok_ref[...] if g is None else xall[g]).astype(F32)
            inverse = lax.rsqrt(jnp.mean(x * x, axis=-1, keepdims=True) + 1e-06)
            normed[pl.ds(i * rows, rows)] = (x * inverse * gain_ref[...]).astype(BF16)
        a = normed[...]

        def dot(w):
            return jnp.dot(a, w[...], preferred_element_type=F32).astype(BF16)

        def put(dst, value):
            for i, g in enumerate(groups):
                g = t if g is None else g
                dst[pl.ds(pl.multiple_of(g * rows, rows), rows)] = value[i * rows : (i + 1) * rows]

        if offset:
            pass
        else:
            for load in loads:
                load.wait()
        put(kv.at[sp, 0], dot(wk))
        put(kv.at[sp, 1], dot(wv))
        put(q_sc, dot(wq))
        put(prod_sc, (dot(wc).astype(F32) * dot(wu).astype(F32)).astype(BF16))
        put(gate_sc, dot(wb))

    to_near.wait_recv()
    project((None, near), 0)
    for c in range(2):
        to_far[c].wait_recv()
        relay[c].start()
    serve(wo, w_sem, own_w, 1)
    for c in range(2):
        relay[c].wait_recv()
    project((far, diag), 1)
    open_ring(kv, kv_sem, None)
    halo = push(prod_sc.at[pl.ds(toks - HALO, HALO)], prev, halo_sem.at[0], halo_sem.at[1], {"sp": following})
    halo.start()

    halo.wait_recv()
    ext[pl.ds(HALO, toks)] = prod_sc[...].astype(F32)
    ext[pl.ds(0, HALO)] = jnp.where(sp == 0, 0.0, prev[...].astype(F32))
    summed = jnp.zeros((toks, ext.shape[1]), F32)
    for tap in range(CONV_K):
        summed = summed + taps_ref[tap : tap + 1, :] * ext[pl.ds(HALO - (CONV_K - 1) + tap, toks)]
    ext[pl.ds(HALO, toks)] = gate_sc[...].astype(F32) * summed
    order = (t, far, near, diag)
    for i, g in enumerate(order):
        conv[pl.ds(i * rows, rows)] = ext[pl.ds(pl.multiple_of(HALO + g * rows, HALO), rows)].astype(BF16)

    for step in range(1, n // 2 + 1):
        serve(kv, kv_sem, None, step)
    if n // 2 >= 2:
        serve(wo, w_sem, own_w, 2)

    key_i = lax.broadcasted_iota(jnp.int32, (toks, toks), 0)
    key_j = lax.broadcasted_iota(jnp.int32, (toks, toks), 1)
    later = (key_i > key_j).astype(F32).astype(BF16)
    causal = key_j < key_i
    scale = HEAD_DIM ** (-0.5)
    for h in range(heads):
        cols = pl.ds(h * HEAD_DIM, HEAD_DIM)
        kv_at = pl.ds((h // grouping) * HEAD_DIM, HEAD_DIM)
        q = q_sc[:, cols]
        shift = shift_ref[0, h]

        def visit(slot, masked, acc, suffix, q=q, shift=shift, kv_at=kv_at):
            z = lax.dot_general(q, kv[slot, 0, :, kv_at], NT, preferred_element_type=F32) * scale + shift
            soft = softplus(z)
            if masked:
                soft = jnp.where(causal, soft, 0.0)
            high = soft.astype(BF16)
            low = (soft - high.astype(F32)).astype(BF16)
            after = jnp.dot(high, later, preferred_element_type=F32) + jnp.dot(low, later, preferred_element_type=F32)
            weight = jnp.exp(z - soft - after - suffix)
            if masked:
                weight = jnp.where(causal, weight, 0.0)
            acc = acc + jnp.dot(weight.astype(BF16), kv[slot, 1, :, kv_at], preferred_element_type=F32)
            return acc, suffix + after[:, 0:1] + soft[:, 0:1]

        acc, suffix = visit(sp, True, jnp.zeros((toks, HEAD_DIM), F32), jnp.zeros((toks, 1), F32))
        acc, suffix = lax.fori_loop(
            0, sp, lambda i, c, visit=visit: visit(sp - 1 - i, False, c[0], c[1]), (acc, suffix)
        )
        ext[pl.ds(HALO, toks), cols] = acc
        logw_ref[:, h : h + 1] = jnp.log(jnp.maximum(1.0 - jnp.exp(-suffix), 0.05))
    for i, g in enumerate(order):
        attn[pl.ds(i * rows, rows)] = ext[pl.ds(pl.multiple_of(HALO + g * rows, HALO), rows), 0 : attn.shape[1]].astype(BF16)

    def block_of(i):
        return ring(pos - (i + 1) // 2) if i % 2 else ring(pos + i // 2)

    def d2d_copy(i):
        return push(snd.at[i], d2d.at[i], d2d_sem.at[0, i], d2d_sem.at[1, i], {"tp": near})

    def x_copy(i):
        return push(xsnd.at[i], xrcv.at[i], x_sem.at[0, i], x_sem.at[1, i], {"tp": far})

    def first(i):
        j = block_of(i)
        wa, wc_ = (woa_ref[...], woc_ref[...]) if i == 0 else (wo[j, 0], wo[j, 1])
        share = lax.dot_general(attn[...], wa, NT, preferred_element_type=F32)
        share = (share + lax.dot_general(conv[...], wc_, NT, preferred_element_type=F32)).astype(BF16)
        snd[i] = share[2 * rows :]
        keep[i] = share[: 2 * rows]
        d2d_copy(i).start()

    def second(i):
        d2d_copy(i).wait_recv()
        xsnd[i] = (keep[i, pl.ds(rows, rows)].astype(F32) + d2d[i, pl.ds(rows, rows)].astype(F32)).astype(BF16)
        x_copy(i).start()

    def third(i):
        x_copy(i).wait_recv()
        own = keep[i, pl.ds(0, rows)].astype(F32) + d2d[i, pl.ds(0, rows)].astype(F32)
        out_ref[block_of(i)] = (own + xrcv[i].astype(F32)).astype(BF16)

    served = 2
    for i in range(n):
        need = (i + 1) // 2
        if need > served:
            serve(wo, w_sem, own_w, need)
            served = need
        first(i)
        if i >= 1:
            second(i - 1)
        if i >= 3:
            third(i - 3)
    second(n - 1)
    for i in range(max(n - 3, 0), n):
        third(i)

    for copy in (*to_far, to_near, *relay, halo):
        copy.wait_send()
    for buf, sem, own in ((wo, w_sem, own_w), (kv, kv_sem, None)):
        for k in range(n - 1):
            for way in range(2):
                hop(buf, sem, way, k, own).wait_send()
    for i in range(n):
        d2d_copy(i).wait_send()
        x_copy(i).wait_send()


def local(
    n, tokens, norm_gain, w_query, w_key, w_value, score_shift, w_conv_b, w_conv_c, w_conv_u,
    conv_kernel, w_out_att, w_out_conv,
):
    rows, d = tokens.shape
    toks = 4 * rows
    feats, att_cols = w_out_att.shape
    conv_cols = w_out_conv.shape[1]
    heads = score_shift.shape[0]
    kv_cols = w_key.shape[1]
    vmem = pl.BlockSpec(memory_space=pltpu.VMEM)
    smem = pl.BlockSpec(memory_space=pltpu.SMEM)
    hbm = pl.BlockSpec(memory_space=pl.ANY)
    dma = pltpu.SemaphoreType.DMA
    out, logw = pl.pallas_call(
        functools.partial(kernel, n),
        out_shape=(
            jax.ShapeDtypeStruct((n, rows, feats), BF16),
            jax.ShapeDtypeStruct((toks, heads), F32),
        ),
        in_specs=[vmem, vmem, hbm, hbm, hbm, smem, hbm, hbm, hbm, vmem, vmem, vmem],
        out_specs=(vmem, vmem),
        scratch_shapes=[
            *[pltpu.VMEM(w.shape, BF16) for w in (w_query, w_key, w_value, w_conv_b, w_conv_c, w_conv_u)],
            pltpu.VMEM((4, rows, d), BF16),
            pltpu.VMEM((2 * rows, d), BF16),
            pltpu.VMEM((toks, w_query.shape[1]), BF16),
            pltpu.VMEM((n, 2, toks, kv_cols), BF16),
            pltpu.VMEM((n, 2, feats, att_cols), BF16),
            pltpu.VMEM((toks, conv_cols), BF16),
            pltpu.VMEM((toks, conv_cols), BF16),
            pltpu.VMEM((HALO, conv_cols), BF16),
            pltpu.VMEM((toks + HALO, max(conv_cols, att_cols)), F32),
            pltpu.VMEM((toks, att_cols), BF16),
            pltpu.VMEM((toks, conv_cols), BF16),
            pltpu.VMEM((n, 2 * rows, feats), BF16),
            pltpu.VMEM((n, 2 * rows, feats), BF16),
            pltpu.VMEM((n, 2 * rows, feats), BF16),
            pltpu.VMEM((n, rows, feats), BF16),
            pltpu.VMEM((n, rows, feats), BF16),
            dma((6,)), dma((5,)), dma((5,)), dma((2, 2, n - 1)), dma((2, 2, n - 1)), dma((2,)), dma((2, n)), dma((2, n)),
        ],
        compiler_params=pltpu.CompilerParams(
            collective_id=0, has_side_effects=True, vmem_limit_bytes=60 * 1024 * 1024
        ),
    )(
        tokens, norm_gain.reshape(1, d), w_query, w_key, w_value, score_shift.reshape(1, heads),
        w_conv_b, w_conv_c, w_conv_u, conv_kernel, w_out_att, w_out_conv,
    )
    return (out.transpose(1, 0, 2).reshape(rows, n * feats), logw)


def solution(mesh):
    return jax.shard_map(
        functools.partial(local, mesh.shape["sp"]),
        mesh=mesh,
        in_specs=(
            P(("sp", "tp"), None), P(), P(None, "tp"), P(None, "tp"), P(None, "tp"), P("tp"),
            P(None, "tp"), P(None, "tp"), P(None, "tp"), P(None, "tp"), P("sp", "tp"), P("sp", "tp"),
        ),
        out_specs=(P(("sp", "tp"), None), P("sp", "tp")),
        check_vma=False,
    )
```

time: 196 us -> 79.5 us (0.41); the launches traced: 194 us -> 79.3 us
  Pallas kernels: 0 us -> 75.2 us
  waiting for transfers between devices: 60 us -> 0 us
  blocking collectives: 46.9 us -> 0 us
  matrix products: 24.6 us -> 0 us
  between operations: 19.2 us -> 0.64 us
  other arithmetic: 17.5 us -> 0 us
  starting transfers between devices: 16.8 us -> 0 us
  local copies, waits for them, and re-layouts: 7.98 us -> 3.44 us
    pallas_call x0 -> x1, Pallas kernels: none -> 75.2 us  [local(): pl.pallas_call(functools.partial(kernel, n), out_shape=(jax.ShapeDtypeStr...]
    all_gather x2 -> x0, blocking collectives: 46.9 us -> none  [the longest x1 24.1 us: local(): lax.all_gather(values, 'sp', axis=0, tiled=True)]
    reduce_scatter x1 -> x0, waiting for transfers between devices: 31.4 us -> none  [local(): lax.psum_scatter(rounded.astype(jnp.bfloat16), 'tp', scatter_dimension=0,...]
    dot_general x13 -> x0, matrix products: 24.6 us -> none  [the longest x5 6.71 us: project(): jnp.dot(normed, weight, preferred_element_type=jnp.float32)]
    all_gather x3 -> x0, waiting for transfers between devices: 20.5 us -> none  [the longest x1 16.9 us: local(): projected = project(lax.all_gather(tokens, 'tp', axis=0, tiled=True))]
    ppermute x10 -> x0, starting transfers between devices: 16.6 us -> none  [the longest x9 13.9 us: swapped(): return lax.ppermute(block, axis, route)]
    another operation x7 -> x0, other arithmetic: 7.65 us -> none
    ppermute x10 -> x0, waiting for transfers between devices: 6.02 us -> none  [the longest x9 6.02 us: swapped(): return lax.ppermute(block, axis, route)]
  transfers between devices with their start and end apart: 14 -> 0, of which waited for: 6 -> 0; matrix products, arithmetic and copies ran while one was open for 21% -> 0% of each run, Pallas kernels for 0% -> 0%
where the time goes in v1:
time: 79.5 us; the launch traced here: 79.3 us
  Pallas kernels  75.2 us (95%)
  local copies, waits for them, and re-layouts  3.44 us (4%)
    pallas_call x1, Pallas kernels, local(): pl.pallas_call(functools.partial(kernel, n), out_shape=(jax.ShapeDtypeStr...  75.2 us
    reshape x1, local copies, waits for them, and re-layouts, local(): return (out.transpose(1, 0, 2).reshape(rows, n * feats), logw)  1.88 us

profile of v1, /device:TPU:17, one launch (start us, length us, event | category | flops | bytes accessed | tf_op | source)
XLA Modules:
  0.0 79.3 jit_solution(9324653197436116656)
XLA Ops:
  0.6 75.2 %shard_map.131 = (bf16[8,64,512]{2,1,0:T(8,128)(2,1)}, f32[256,2]{1,0:T(8,128)}) custom-call(bf16[64,4096]{1,0:T(8,128)(2,1)} %tok_ref.1, f32[1,4096]{1,0:T(1,128)} %bitcast.7, bf16[4096,256]{1,0:T(8,128)(2,1)} %wq_hbm.1, bf16[4096,128]{1,0:T(8,128)(2,1)} %wk_hbm.1, bf16[4096,128]{1,0:T(8,128)(2,1)} %wv_hbm.1, f32[1,2]{1,0:T(1,128)} %bitcast.8, ...), custom_call_target="tpu_custom_call" | custom-call | tf_op jit(solution)/shard_map/pallas_call | solution.py:266
  75.8 1.9 %copy.17 = bf16[8,8,8,512]{3,2,0,1:T(8,128)(2,1)} copy(bf16[8,8,8,512]{3,2,1,0:T(8,128)(2,1)} %bitcast.6) | data formatting | bytes 1048576 | tf_op jit(solution)/shard_map/reshape | solution.py:301
  77.7 1.6 %copy.16 = f32[256,2]{0,1:T(2,128)} copy(f32[256,2]{1,0:T(8,128)} %get-tuple-element.9) | data formatting | bytes 4096

commit v2 on v1

v2 whole, which is shorter than its diff:
```python
import functools

import jax
import jax.numpy as jnp
from jax import lax
from jax.experimental import pallas as pl
from jax.experimental.pallas import tpu as pltpu
from jax.sharding import PartitionSpec as P

HEAD_DIM = 128
CONV_K = 3
HALO = 16
F32 = jnp.float32
BF16 = jnp.bfloat16
MESH = pl.DeviceIdType.MESH
NT = (((1,), (1,)), ((), ()))


def softplus(z):
    u = jnp.exp(-jnp.abs(z))
    small = u * (1.0 - u * (0.5 - u * (1.0 / 3.0 - u * 0.25)))
    return jnp.maximum(z, 0.0) + jnp.where(u < 0.01, small, jnp.log(1.0 + u))


def kernel(
    n,
    tok_ref, gain_ref, wq_hbm, wk_hbm, wv_hbm, shift_ref, wb_hbm, wc_hbm, wu_hbm, taps_ref, woa_ref, woc_ref,
    out_ref, logw_ref,
    wq, wk, wv, wb, wc, wu, xall, normed, q_sc, kv, wo, gate_sc, prod_sc, prev, ext, attn, conv, partial, totals,
    snd, keep, d2d, xsnd, xrcv,
    load_sem, tok_ssem, tok_rsem, kv_sem, w_sem, halo_sem, d2d_sem, x_sem,
):
    sp = lax.axis_index("sp")
    t = lax.axis_index("tp")
    near = t + 1 - 2 * (t % 2)
    far = t + 2 - 4 * ((t // 2) % 2)
    diag = near + 2 - 4 * ((near // 2) % 2)
    pos = jnp.where(sp % 2 == 0, sp // 2, n - 1 - sp // 2)

    def ring(place):
        place = (place + 2 * n) % n
        return jnp.where(place < n // 2, 2 * place, 2 * (n - 1 - place) + 1)

    right, left = ring(pos + 1), ring(pos - 1)
    following, leading = (sp + 1) % n, (sp + n - 1) % n
    rows = tok_ref.shape[0]
    toks = 4 * rows
    half = rows // 2
    fpart = wo.shape[2] // 2
    heads = q_sc.shape[1] // HEAD_DIM
    kv_cols = kv.shape[4]
    grouping = heads // (kv_cols // HEAD_DIM)

    loads = [
        pltpu.make_async_copy(src, dst, load_sem.at[i])
        for i, (src, dst) in enumerate(
            ((wk_hbm, wk), (wv_hbm, wv), (wq_hbm, wq), (wc_hbm, wc), (wu_hbm, wu), (wb_hbm, wb))
        )
    ]
    own_loads = [
        pltpu.make_async_copy(src, wo.at[sp, i], load_sem.at[6 + i]) for i, src in enumerate((woa_ref, woc_ref))
    ]
    barrier = pltpu.get_barrier_semaphore()
    for place in (right, left, following, leading):
        pl.semaphore_signal(barrier, inc=1, device_id={"sp": place}, device_id_type=MESH)
    for place in (near, far):
        pl.semaphore_signal(barrier, inc=1, device_id={"tp": place}, device_id_type=MESH)
    for load in (*own_loads, *loads):
        load.start()
    pl.semaphore_wait(barrier, 6)

    def push(src, dst, ssem, rsem, who):
        return pltpu.make_async_remote_copy(
            src_ref=src, dst_ref=dst, send_sem=ssem, recv_sem=rsem, device_id=who, device_id_type=MESH
        )

    to_far = [
        push(tok_ref.at[pl.ds(c * half, half)], xall.at[t, pl.ds(c * half, half)], tok_ssem.at[c], tok_rsem.at[c], {"tp": far})
        for c in range(2)
    ]
    to_near = push(tok_ref, xall.at[t], tok_ssem.at[2], tok_rsem.at[2], {"tp": near})
    relay = [
        push(xall.at[far, pl.ds(c * half, half)], xall.at[far, pl.ds(c * half, half)], tok_ssem.at[3 + c], tok_rsem.at[3 + c], {"tp": near})
        for c in range(2)
    ]
    for copy in to_far:
        copy.start()
    to_near.start()

    last = n // 2

    def hop(part, sem, way, step, chunk):
        block = ring(pos - (step - 1)) if way == 0 else ring(pos + (step - 1))
        view = part(block, chunk, step)
        return push(
            view[0], view[1], sem.at[0, way, step - 1, chunk], sem.at[1, way, step - 1, chunk],
            {"sp": right if way == 0 else left},
        )

    def ways(step, chunk, chunks):
        if isinstance(step, int) and step == last:
            return (0,) if chunk < chunks // 2 else (1,)
        return (0, 1)

    early = t // 2

    def kv_part(block, chunk, step):
        view = kv.at[block, early + chunk * (1 - 2 * early)]
        return view, view

    def w_part(block, chunk, step):
        view = wo.at[block, chunk // 2, pl.ds(pl.multiple_of((chunk % 2) * fpart, fpart), fpart)]
        return view, view

    rings = {"kv": (kv_part, kv_sem, 2), "w": (w_part, w_sem, 4)}

    def emit(name, step, chunk):
        part, sem, chunks = rings[name]
        for way in ways(step, chunk, chunks):
            hop(part, sem, way, step, chunk).start()

    def take(name, step, chunk, onward=None):
        part, sem, chunks = rings[name]
        for way in ways(step, chunk, chunks):
            hop(part, sem, way, step, chunk).wait_recv()
        if onward or (onward is None and step < last):
            emit(name, step + 1, chunk)

    for load in own_loads:
        load.wait()
    for chunk in (0, 1):
        emit("w", 1, chunk)

    def dot(w):
        return jnp.dot(normed[...], w[...], preferred_element_type=F32).astype(BF16)

    def project_kv(groups, pair):
        for i, g in enumerate(groups):
            x = (tok_ref[...] if g is None else xall[g]).astype(F32)
            inverse = lax.rsqrt(jnp.mean(x * x, axis=-1, keepdims=True) + 1e-06)
            at = rows * (t % 2 if i == 0 else 1 - t % 2)
            normed[pl.ds(pl.multiple_of(at, rows), rows)] = (x * inverse * gain_ref[...]).astype(BF16)
        kv[sp, pair, 0] = dot(wk)
        kv[sp, pair, 1] = dot(wv)

    def project_rest(pair):
        at = pl.ds(pl.multiple_of(pair * 2 * rows, 2 * rows), 2 * rows)
        prod_sc[at] = (dot(wc).astype(F32) * dot(wu).astype(F32)).astype(BF16)
        q_sc[at] = dot(wq)
        gate_sc[at] = dot(wb)

    to_near.wait_recv()
    for load in loads[:2]:
        load.wait()
    project_kv((None, near), early)
    emit("kv", 1, 0)
    for chunk in (2, 3):
        emit("w", 1, chunk)
    for load in loads[2:]:
        load.wait()
    project_rest(early)
    to_far[0].wait_recv()
    relay[0].start()
    take("kv", 1, 0)
    take("w", 1, 0)
    to_far[1].wait_recv()
    relay[1].start()
    for c in range(2):
        relay[c].wait_recv()
    project_kv((far, diag), 1 - early)
    emit("kv", 1, 1)
    take("w", 1, 1)
    project_rest(1 - early)
    halo = push(prod_sc.at[pl.ds(toks - HALO, HALO)], prev, halo_sem.at[0], halo_sem.at[1], {"sp": following})
    halo.start()

    key_i = lax.broadcasted_iota(jnp.int32, (toks, toks), 0)
    key_j = lax.broadcasted_iota(jnp.int32, (toks, toks), 1)
    later = (key_i > key_j).astype(F32).astype(BF16)
    lane = lax.broadcasted_iota(jnp.int32, (toks, totals.shape[2]), 1)
    scale = HEAD_DIM ** (-0.5)
    order = (t, far, near, diag)

    def visit(slot, masked):
        for h in range(heads):
            cols = pl.ds(h * HEAD_DIM, HEAD_DIM)
            kv_at = pl.ds((h // grouping) * HEAD_DIM, HEAD_DIM)
            keys = kv[slot, :, 0, :, kv_at].reshape(toks, HEAD_DIM)
            vals = kv[slot, :, 1, :, kv_at].reshape(toks, HEAD_DIM)
            z = lax.dot_general(q_sc[:, cols], keys, NT, preferred_element_type=F32) * scale + shift_ref[0, h]
            soft = softplus(z)
            if masked:
                soft = jnp.where(key_j < key_i, soft, 0.0)
            high = soft.astype(BF16)
            low = (soft - high.astype(F32)).astype(BF16)
            after = jnp.dot(high, later, preferred_element_type=F32) + jnp.dot(low, later, preferred_element_type=F32)
            weight = jnp.exp(z - soft - after)
            if masked:
                weight = jnp.where(key_j < key_i, weight, 0.0)
            partial[slot, :, cols] = jnp.dot(weight.astype(BF16), vals, preferred_element_type=F32)
            total = after[:, 0:1] + soft[:, 0:1]
            totals[h] = jnp.where(lane == slot, total, totals[h])

    def visit_at(step, both=True):
        def side(i, carry):
            slot = ring(pos + (2 * i - 1) * step)

            @pl.when(slot < sp)
            def _():
                visit(slot, False)

            return carry

        lax.fori_loop(0, 2 if both else 1, side, 0)

    totals[...] = jnp.zeros(totals.shape, F32)
    visit(sp, True)

    def w_event(m):
        return m // 4 + 1, m % 4

    def body(s, carry):
        if n > 4:
            take("kv", s + 1, 0, True)
            take("kv", s, 1, True)
            visit_at(s)
            take("w", *w_event(2 * s), True)
            take("w", *w_event(2 * s + 1), True)
        return carry

    def convolve():
        halo.wait_recv()
        ext[pl.ds(HALO, toks)] = prod_sc[...].astype(F32)
        ext[pl.ds(0, HALO)] = jnp.where(sp == 0, 0.0, prev[...].astype(F32))
        summed = jnp.zeros((toks, ext.shape[1]), F32)
        for tap in range(CONV_K):
            summed = summed + taps_ref[tap : tap + 1, :] * ext[pl.ds(HALO - (CONV_K - 1) + tap, toks)]
        ext[pl.ds(HALO, toks)] = gate_sc[...].astype(F32) * summed
        for i, g in enumerate(order):
            conv[pl.ds(i * rows, rows)] = ext[pl.ds(pl.multiple_of(HALO + g * rows, HALO), rows)].astype(BF16)

    loops = max(last - 3, 0)
    lax.fori_loop(1, 1 + loops, body, 0)
    w_done = 2 + 2 * loops
    convolve()
    for s in range(1 + loops, last + 1):
        if s + 1 <= last:
            take("kv", s + 1, 0)
        take("kv", s, 1)
        visit_at(s, s < last)
        if s < last:
            for m in (w_done, w_done + 1):
                take("w", *w_event(m))
            w_done += 2

    def combine(i, carry):
        slot = sp - i
        suffixes = []
        for h in range(heads):
            cols = pl.ds(h * HEAD_DIM, HEAD_DIM)
            suffix = carry[h]
            ext[pl.ds(HALO, toks), cols] += jnp.exp(-suffix) * partial[slot, :, cols]
            total = jnp.sum(jnp.where(lane == slot, totals[h], 0.0), axis=1, keepdims=True)
            suffixes.append(suffix + total)
        return tuple(suffixes)

    ext[...] = jnp.zeros(ext.shape, F32)
    suffixes = lax.fori_loop(0, sp + 1, combine, tuple(jnp.zeros((toks, 1), F32) for _ in range(heads)))
    for h in range(heads):
        spread = jnp.broadcast_to(suffixes[h], (toks, 128)).T[0:1, :]
        logw_ref[h : h + 1, :] = jnp.log(jnp.maximum(1.0 - jnp.exp(-spread), 0.05))
    for i, g in enumerate(order):
        attn[pl.ds(i * rows, rows)] = ext[pl.ds(pl.multiple_of(HALO + g * rows, HALO), rows), 0 : attn.shape[1]].astype(BF16)

    def block_of(i):
        return ring(pos - (i + 1) // 2) if i % 2 else ring(pos + i // 2)

    def d2d_copy(i):
        return push(snd.at[i], d2d.at[i], d2d_sem.at[0, i], d2d_sem.at[1, i], {"tp": near})

    def x_copy(i):
        return push(xsnd.at[i], xrcv.at[i], x_sem.at[0, i], x_sem.at[1, i], {"tp": far})

    def first(i):
        j = block_of(i)
        share = lax.dot_general(attn[...], wo[j, 0], NT, preferred_element_type=F32)
        share = (share + lax.dot_general(conv[...], wo[j, 1], NT, preferred_element_type=F32)).astype(BF16)
        snd[i] = share[2 * rows :]
        keep[i] = share[: 2 * rows]
        d2d_copy(i).start()

    def second(i):
        d2d_copy(i).wait_recv()
        xsnd[i] = (keep[i, pl.ds(rows, rows)].astype(F32) + d2d[i, pl.ds(rows, rows)].astype(F32)).astype(BF16)
        x_copy(i).start()

    def third(i):
        x_copy(i).wait_recv()
        own = keep[i, pl.ds(0, rows)].astype(F32) + d2d[i, pl.ds(0, rows)].astype(F32)
        done = (own + xrcv[i].astype(F32)).astype(BF16)
        if len(out_ref.shape) == 3:
            out_ref[block_of(i)] = done
        else:
            feats = keep.shape[2]
            out_ref[:, pl.ds(pl.multiple_of(block_of(i) * feats, feats), feats)] = done

    for i in range(n):
        while w_done < 4 * ((i + 1) // 2):
            take("w", *w_event(w_done))
            w_done += 1
        first(i)
        if i >= 1:
            second(i - 1)
        if i >= 3:
            third(i - 3)
    second(n - 1)
    for i in range(max(n - 3, 0), n):
        third(i)

    for copy in (*to_far, to_near, *relay, halo):
        copy.wait_send()
    for part, sem, chunks in rings.values():
        for step in range(1, last + 1):
            for chunk in range(chunks):
                for way in ways(step, chunk, chunks):
                    hop(part, sem, way, step, chunk).wait_send()
    for i in range(n):
        d2d_copy(i).wait_send()
        x_copy(i).wait_send()


def local(
    n, tokens, norm_gain, w_query, w_key, w_value, score_shift, w_conv_b, w_conv_c, w_conv_u,
    conv_kernel, w_out_att, w_out_conv,
):
    rows, d = tokens.shape
    toks = 4 * rows
    feats, att_cols = w_out_att.shape
    conv_cols = w_out_conv.shape[1]
    heads = score_shift.shape[0]
    kv_cols = w_key.shape[1]
    vmem = pl.BlockSpec(memory_space=pltpu.VMEM)
    smem = pl.BlockSpec(memory_space=pltpu.SMEM)
    hbm = pl.BlockSpec(memory_space=pl.ANY)
    dma = pltpu.SemaphoreType.DMA
    wide = feats % 128 == 0
    out, logw = pl.pallas_call(
        functools.partial(kernel, n),
        out_shape=(
            jax.ShapeDtypeStruct((rows, n * feats) if wide else (n, rows, feats), BF16),
            jax.ShapeDtypeStruct((heads, toks), F32),
        ),
        in_specs=[vmem, vmem, hbm, hbm, hbm, smem, hbm, hbm, hbm, vmem, hbm, hbm],
        out_specs=(vmem, vmem),
        scratch_shapes=[
            *[pltpu.VMEM(w.shape, BF16) for w in (w_query, w_key, w_value, w_conv_b, w_conv_c, w_conv_u)],
            pltpu.VMEM((4, rows, d), BF16),
            pltpu.VMEM((2 * rows, d), BF16),
            pltpu.VMEM((toks, w_query.shape[1]), BF16),
            pltpu.VMEM((n, 2, 2, 2 * rows, kv_cols), BF16),
            pltpu.VMEM((n, 2, feats, att_cols), BF16),
            pltpu.VMEM((toks, conv_cols), BF16),
            pltpu.VMEM((toks, conv_cols), BF16),
            pltpu.VMEM((HALO, conv_cols), BF16),
            pltpu.VMEM((toks + HALO, max(conv_cols, att_cols)), F32),
            pltpu.VMEM((toks, att_cols), BF16),
            pltpu.VMEM((toks, conv_cols), BF16),
            pltpu.VMEM((n, toks, att_cols), F32),
            pltpu.VMEM((heads, toks, 128), F32),
            pltpu.VMEM((n, 2 * rows, feats), BF16),
            pltpu.VMEM((n, 2 * rows, feats), BF16),
            pltpu.VMEM((n, 2 * rows, feats), BF16),
            pltpu.VMEM((n, rows, feats), BF16),
            pltpu.VMEM((n, rows, feats), BF16),
            dma((8,)), dma((5,)), dma((5,)), dma((2, 2, n // 2, 2)), dma((2, 2, n // 2, 4)), dma((2,)), dma((2, n)), dma((2, n)),
        ],
        compiler_params=pltpu.CompilerParams(
            collective_id=0, has_side_effects=True, vmem_limit_bytes=60 * 1024 * 1024
        ),
    )(
        tokens, norm_gain.reshape(1, d), w_query, w_key, w_value, score_shift.reshape(1, heads),
        w_conv_b, w_conv_c, w_conv_u, conv_kernel, w_out_att, w_out_conv,
    )
    if not wide:
        out = out.transpose(1, 0, 2).reshape(rows, n * feats)
    return (out, logw.T)


def solution(mesh):
    return jax.shard_map(
        functools.partial(local, mesh.shape["sp"]),
        mesh=mesh,
        in_specs=(
            P(("sp", "tp"), None), P(), P(None, "tp"), P(None, "tp"), P(None, "tp"), P("tp"),
            P(None, "tp"), P(None, "tp"), P(None, "tp"), P(None, "tp"), P("sp", "tp"), P("sp", "tp"),
        ),
        out_specs=(P(("sp", "tp"), None), P("sp", "tp")),
        check_vma=False,
    )
```

time: 79.5 us -> 72.9 us (0.917); the launches traced: 79.3 us -> 71.8 us
  Pallas kernels: 75.2 us -> 68 us
    pallas_call x1, Pallas kernels: 75.2 us -> 68 us  [local(): pl.pallas_call(functools.partial(kernel, n), out_shape=(jax.ShapeDtypeStr...]
    reshape x1 -> x0, local copies, waits for them, and re-layouts: 1.88 us -> none  [local(): return (out.transpose(1, 0, 2).reshape(rows, n * feats), logw)]
    unnamed x1 -> x2, local copies, waits for them, and re-layouts: 1.56 us -> 3.12 us
where the time goes in v2:
time: 72.9 us; the launch traced here: 71.8 us
  Pallas kernels  68 us (93%)
  local copies, waits for them, and re-layouts  3.12 us (4%)
    pallas_call x1, Pallas kernels, local(): pl.pallas_call(functools.partial(kernel, n), out_shape=(jax.ShapeDtypeStr...  68 us
    unnamed x2, local copies, waits for them, and re-layouts  3.12 us

profile of v2, /device:TPU:17, one launch (start us, length us, event | category | flops | bytes accessed | tf_op | source)
XLA Modules:
  0.0 71.8 jit_solution(8133265186414063459)
XLA Ops:
  0.6 68.0 %shard_map.131 = (bf16[64,4096]{1,0:T(8,128)(2,1)}, f32[2,256]{1,0:T(2,128)}) custom-call(bf16[64,4096]{1,0:T(8,128)(2,1)} %tok_ref.1, f32[1,4096]{1,0:T(1,128)} %bitcast.3, bf16[4096,256]{1,0:T(8,128)(2,1)} %wq_hbm.1, bf16[4096,128]{1,0:T(8,128)(2,1)} %wk_hbm.1, bf16[4096,128]{1,0:T(8,128)(2,1)} %wv_hbm.1, f32[1,2]{1,0:T(1,128)} %bitcast.5, ...), custom_call_target="tpu_custom_call" | custom-call | tf_op jit(solution)/shard_map/pallas_call | solution.py:347
  68.7 1.9 %copy.16 = bf16[64,4096]{1,0:T(8,128)(2,1)} copy(bf16[64,4096]{1,0:T(8,128)(2,1)} %get-tuple-element.8) | data formatting | bytes 1048576
  70.6 1.3 %copy.17 = f32[256,2]{0,1:T(2,128)} copy(f32[256,2]{0,1:T(2,128)} %bitcast.4) | data formatting | bytes 4096
